TPU v7x, 128 devices: a whole 4x4x4 slice. The times are simulated.
128 devices in a mesh: ep: 128 (over z, y, x, core).
Axes of the slice: x: 4, y: 4, z: 4, core: 2. Of those that a mesh axis runs over, the one named last changes fastest.
Arguments:
- tokens: bfloat16 [512, 4, 1024], P('ep'), may hold values from -6 to 6
- lengths: int32 [512], P('ep'), may hold values from 1 to 4, 768 in all
- routes: int32 [512, 4, 8], P('ep'), may hold values from 0 to 255, all different within a row; in each aligned block of 16 rows (0 to 15, 16 to 31, ...) at most 4 rows name the same one
- gates: float32 [512, 4, 8], P('ep'), may hold values from 0.05 to 0.6
- norm_gain: float32 [1024], replicated, may hold values from 0.5 to 1.5
- expert_gate: bfloat16 [256, 1024, 256], P('ep'), may hold values from -0.1875 to 0.1875
- expert_up: bfloat16 [256, 1024, 256], P('ep'), may hold values from -0.1875 to 0.1875
- expert_down: bfloat16 [256, 256, 1024], P('ep'), may hold values from -0.375 to 0.375
- shared_gate: bfloat16 [1024, 256], replicated, may hold values from -0.1875 to 0.1875
- shared_up: bfloat16 [1024, 256], replicated, may hold values from -0.1875 to 0.1875
- shared_down: bfloat16 [256, 1024], replicated, may hold values from -0.375 to 0.375
- out_gain: float32 [1024], replicated, may hold values from 0.5 to 1.5
Outputs:
- mixed: bfloat16 [512, 4, 1024], P('ep')
Inputs may be any that keep to these rules, and one draw needn't show every extreme that they name: `routes`: in the 16 rows of one device (all slots, in order), no expert is named by more than 4 rows, and some device reaches 4; the experts of one row differ. `lengths`: each sequence has 1 to 4 live slots, the longest exactly 4.
All inputs are finite; a program needn't handle non-finite values.
Results may differ from a plain program's by a relative error of at most 0.0065.
Values may be sent and summed in bfloat16 or wider, within the bound.
A program may use at most 64 MiB of HBM per device.

v0:
```python
import jax
import jax.numpy as jnp
from jax import lax
from jax.sharding import PartitionSpec as P

MOST = 4


EPS = 1e-06


def norm_rows(values, scales):
    wide = values.astype(jnp.float32)
    return wide * lax.rsqrt(jnp.mean(wide * wide, axis=-1, keepdims=True) + EPS) * scales


def run_experts(stacked, expert_gate, expert_up, expert_down):
    gate_part = jnp.einsum("erd,edf->erf", stacked, expert_gate, preferred_element_type=jnp.float32)
    up_part = jnp.einsum("erd,edf->erf", stacked, expert_up, preferred_element_type=jnp.float32)
    hidden = (jax.nn.silu(gate_part) * up_part).astype(jnp.bfloat16)
    return jnp.einsum(
        "erf,efd->erd", hidden, expert_down, preferred_element_type=jnp.float32
    ).astype(jnp.bfloat16)


def padded_path(normed, expert_ids, live_mask, weights, expert_gate, expert_up, expert_down):
    token_count, top_count = expert_ids.shape
    features = normed.shape[1]
    local_count = expert_gate.shape[0]
    devices = lax.axis_size("ep")
    experts_all = local_count * devices
    flat_ids = expert_ids.reshape(-1)
    live_rows = jnp.repeat(live_mask, top_count)
    matches = (
        (flat_ids[:, None] == lax.broadcasted_iota(jnp.int32, (1, experts_all), 1))
        & live_rows[:, None]
    ).astype(jnp.int32)
    earlier = jnp.cumsum(matches, axis=0) - matches
    position = jnp.sum(earlier * matches, axis=1)
    targets = jnp.where(live_rows, flat_ids * MOST + position, experts_all * MOST)
    copies = jnp.repeat(normed, top_count, axis=0)
    outgoing = (
        jnp.zeros((experts_all * MOST, features), jnp.bfloat16).at[targets].set(copies, mode="drop")
    )
    outgoing = outgoing.reshape(devices, local_count * MOST, features)
    arrived = lax.all_to_all(outgoing, "ep", split_axis=0, concat_axis=0, tiled=True)
    stacked = (
        arrived.reshape(devices, local_count, MOST, features)
        .transpose(1, 0, 2, 3)
        .reshape(local_count, devices * MOST, features)
    )
    results = run_experts(stacked, expert_gate, expert_up, expert_down)
    replies = (
        results.reshape(local_count, devices, MOST, features)
        .transpose(1, 0, 2, 3)
        .reshape(devices, local_count * MOST, features)
    )
    returned = lax.all_to_all(replies, "ep", split_axis=0, concat_axis=0, tiled=True)
    returned_flat = returned.reshape(experts_all * MOST, features)
    fetched = returned_flat[jnp.minimum(targets, experts_all * MOST - 1)].reshape(
        token_count, top_count, features
    )
    return jnp.sum(weights[:, :, None] * fetched.astype(jnp.float32), axis=1)


def per_device(
    tokens,
    lengths,
    routes,
    gates,
    norm_gain,
    expert_gate,
    expert_up,
    expert_down,
    shared_gate,
    shared_up,
    shared_down,
    out_gain,
):
    seq_count, new_count, features = tokens.shape
    flat_rows = tokens.reshape(seq_count * new_count, features)
    normed = norm_rows(flat_rows, norm_gain).astype(jnp.bfloat16)
    live_mask = (
        lax.broadcasted_iota(jnp.int32, (seq_count, new_count), 1) < lengths[:, None]
    ).reshape(-1)
    expert_ids = routes.reshape(seq_count * new_count, routes.shape[-1])
    weights = jnp.where(live_mask[:, None], gates.reshape(expert_ids.shape), 0.0)
    routed = padded_path(
        normed, expert_ids, live_mask, weights, expert_gate, expert_up, expert_down
    )
    shared_hidden = (
        jax.nn.silu(jnp.dot(normed, shared_gate, preferred_element_type=jnp.float32))
        * jnp.dot(normed, shared_up, preferred_element_type=jnp.float32)
    ).astype(jnp.bfloat16)
    shared = jnp.dot(shared_hidden, shared_down, preferred_element_type=jnp.float32)
    summed = routed + shared
    mixed_out = jnp.where(live_mask[:, None], norm_rows(summed, out_gain), 0.0)
    return mixed_out.astype(jnp.bfloat16).reshape(tokens.shape)


def solution(mesh):
    placed = (
        P("ep", None, None),
        P("ep"),
        P("ep", None, None),
        P("ep", None, None),
        P(),
        P("ep", None, None),
        P("ep", None, None),
        P("ep", None, None),
        P(),
        P(),
        P(),
        P(),
    )
    return jax.shard_map(
        per_device, mesh=mesh, in_specs=placed, out_specs=P("ep", None, None), check_vma=False
    )
```

profile of v0, /device:TPU:0, one launch (start us, length us, event | category | flops | bytes accessed | tf_op | source)
XLA Modules:
  0.0 112.4 jit_solution(12069191260470576875)
XLA Ops:
  0.0 0.8 iota_compare_fusion.1
  1.2 0.8 eq.15
  2.0 0.7 broadcast_multiply_fusion
  2.7 0.8 reshape.174
  3.4 0.9 multiply_reduce_fusion.1
  4.4 0.2 reduce_window_sum.11
  5.0 0.8 multiply_convert_fusion
  5.8 1.9 %scatter_custom_fusion = bf16[1024,1024]{1,0:T(8,128)(2,1)S(1)} fusion(s32[128]{0:T(128)S(1)} %get-tuple-element.6, bf16[]{:T(256)} %constant.10.clone.1, bf16[16,1024]{1,0:T(8,128)(2,1)S(1)} %multiply_convert_fusion), kind=kCustom, calls=%fused_computation.13 | custom fusion | bytes 2129922 | tf_op jit(solution)/shard_map/scatter | solution.py:43
  7.6 42.9 %all_to_all.10 = bf16[128,8,1024]{2,1,0:T(8,128)(2,1)S(1)} all-to-all(bf16[128,8,1024]{2,1,0:T(8,128)(2,1)S(1)} %bitcast.38), channel_id=1, replica_groups=mesh['ep'=128] {'ep'}, dimensions={0} | all-to-all | bytes 4194304 | tf_op jit(solution)/shard_map/all_to_all | solution.py:46
  50.5 1.2 %copy.20 = bf16[128,8,1024]{2,0,1:T(8,128)(2,1)S(1)} copy(bf16[128,8,1024]{2,1,0:T(8,128)(2,1)S(1)} %all_to_all.10) | data formatting | bytes 4194304 | tf_op jit(solution)/shard_map/all_to_all | solution.py:46
  51.7 3.0 %copy.21 = bf16[2,128,4,1024]{3,2,1,0:T(4,128)(2,1)} copy(bf16[2,128,4,1024]{3,1,2,0:T(8,128)(2,1)S(1)} %bitcast.39) | data formatting | bytes 4194304 | tf_op jit(solution)/shard_map/transpose | solution.py:49
  54.6 2.5 %reshape.169 = bf16[2,512,1024]{2,1,0:T(8,128)(2,1)S(1)} reshape(bf16[2,128,4,1024]{3,2,1,0:T(4,128)(2,1)} %copy.21) | data formatting | bytes 4194304 | tf_op jit(solution)/shard_map/reshape | solution.py:50
  57.2 2.9 %fusion.26 = f32[2,512,256]{2,1,0:T(8,128)} fusion(bf16[2,512,1024]{2,1,0:T(8,128)(2,1)S(1)} %reshape.169, bf16[2,1024,256]{2,1,0:T(8,128)(2,1)} %param.17), kind=kOutput, calls=%fused_computation.48 | convolution fusion | flops 536870912 | bytes 4194304 | tf_op jit(solution)/shard_map/erd,edf->erf/dot_general | solution.py:18
  60.1 4.3 %convolution_convert_fusion = bf16[2,512,1024]{2,1,0:T(8,128)(2,1)} fusion(bf16[2,256,1024]{2,1,0:T(8,128)(2,1)S(1)} %copy-done, bf16[2,512,1024]{2,1,0:T(8,128)(2,1)S(1)} %reshape.169, bf16[2,1024,256]{2,1,0:T(8,128)(2,1)} %param.18, f32[2,512,256]{2,1,0:T(8,128)} %fusion.26), kind=kOutput, calls=%fused_computation.2 | convolution fusion | flops 1076363264 | bytes 7340032 | tf_op jit(solution)/shard_map/erf,efd->erd/dot_general | solution.py:21
  64.4 2.7 %reshape.170 = bf16[2,128,4,1024]{3,2,1,0:T(4,128)(2,1)S(1)} reshape(bf16[2,512,1024]{2,1,0:T(8,128)(2,1)} %convolution_convert_fusion) | data formatting | bytes 4194304 | tf_op jit(solution)/shard_map/reshape | solution.py:54
  67.1 0.6 copy.22
  67.8 2.5 %copy.23 = bf16[128,8,1024]{2,1,0:T(8,128)(2,1)} copy(bf16[128,8,1024]{2,0,1:T(8,128)(2,1)S(1)} %bitcast.40) | data formatting | bytes 4194304 | tf_op jit(solution)/shard_map/reshape | solution.py:56
  70.3 4.8 %all-to-all-start.1 = ((bf16[128,8,1024]{2,1,0:T(8,128)(2,1)}), bf16[128,8,1024]{2,1,0:T(8,128)(2,1)S(1)}, u32[]{:S(2)}, u32[]{:S(2)}) async-start(bf16[128,8,1024]{2,1,0:T(8,128)(2,1)} %copy.23), calls=%async_computation.1 | async-start | bytes 4194304 | tf_op jit(solution)/shard_map/all_to_all | solution.py:58
  75.1 1.2 %fusion.27 = f32[16,256]{1,0:T(8,128)S(1)} fusion(bf16[16,1024]{1,0:T(8,128)(2,1)S(1)} %multiply_convert_fusion, bf16[1024,256]{1,0:T(8,128)(2,1)} %param.20), kind=kOutput, calls=%fused_computation.49 | convolution fusion | flops 8388608 | bytes 573440 | tf_op jit(solution)/shard_map/dot_general | solution.py:92
  76.4 32.5 %all-to-all-done.1 = bf16[128,8,1024]{2,1,0:T(8,128)(2,1)S(1)} async-done(((bf16[128,8,1024]{2,1,0:T(8,128)(2,1)}), bf16[128,8,1024]{2,1,0:T(8,128)(2,1)S(1)}, u32[]{:S(2)}, u32[]{:S(2)}) %all-to-all-start.1) | async-done | bytes 2097184 | tf_op jit(solution)/shard_map/all_to_all | solution.py:58
  108.8 0.9 gather_fusion
  109.7 0.2 fusion.9
  109.9 1.8 %multiply_reduce_fusion = (f32[16]{0:T(128)S(1)}, f32[16,1024]{1,0:T(8,128)S(1)}) fusion(f32[16,1024]{1,0:T(8,128)S(1)} %fusion.9, bf16[256,1024]{1,0:T(8,128)(2,1)} %param.22, bf16[16,1024]{1,0:T(8,128)(2,1)S(1)} %multiply_convert_fusion, bf16[1024,256]{1,0:T(8,128)(2,1)} %param.21, f32[16,256]{1,0:T(8,128)S(1)} %fusion.27), kind=kOutput, calls=%fused_computation.25 | convolution fusion | flops 16850928 | bytes 1228864 | tf_op jit(solution)/shard_map/dot_general | solution.py:95
  111.8 0.6 reshape.173
  (20 shorter events, 1.0 us)
Async XLA Ops:
  0.0 60.1 %copy-start = (bf16[2,256,1024]{2,1,0:T(8,128)(2,1)S(1)}, bf16[2,256,1024]{2,1,0:T(8,128)(2,1)}, u32[]{:S(2)}) copy-start(bf16[2,256,1024]{2,1,0:T(8,128)(2,1)} %param.19) | copy-start | bytes 3145732
  70.3 4.8 %copy-start.1 = (f32[4,4,8]{2,1,0:T(4,128)S(1)}, f32[4,4,8]{2,1,0:T(4,128)}, u32[]{:S(2)}) copy-start(f32[4,4,8]{2,1,0:T(4,128)} %param.15) | copy-start | bytes 1540
  70.3 38.6 %all-to-all-start.1 = ((bf16[128,8,1024]{2,1,0:T(8,128)(2,1)}), bf16[128,8,1024]{2,1,0:T(8,128)(2,1)S(1)}, u32[]{:S(2)}, u32[]{:S(2)}) async-start(bf16[128,8,1024]{2,1,0:T(8,128)(2,1)} %copy.23), calls=%async_computation.1 | async-start | bytes 4194304 | tf_op jit(solution)/shard_map/all_to_all | solution.py:58
  76.4 35.4 %copy-start.2 = (f32[1024]{0:T(1024)S(1)}, f32[1024]{0:T(1024)}, u32[]{:S(2)}) copy-start(f32[1024]{0:T(1024)} %param.23) | copy-start | bytes 12292
where the time goes:
time: 114 us; the launch traced here: 112 us
  blocking collectives  42.9 us (38%)
  waiting for transfers between devices  32.5 us (29%)
  local copies, waits for them, and re-layouts  18 us (16%)
  matrix products  10.2 us (9%)
  starting transfers between devices  4.78 us (4%)
  other arithmetic  4.01 us (4%)
    all_to_all x1, blocking collectives, padded_path(): lax.all_to_all(outgoing, 'ep', split_axis=0, concat_axis=0, tiled=True)  42.9 us
    all_to_all x1, waiting for transfers between devices, padded_path(): lax.all_to_all(replies, 'ep', split_axis=0, concat_axis=0, tiled=True)  32.5 us
    all_to_all x1, starting transfers between devices, padded_path(): lax.all_to_all(replies, 'ep', split_axis=0, concat_axis=0, tiled=True)  4.78 us
    dot_general x1, matrix products, run_experts(): jnp.einsum('erf,efd->erd', hidden, expert_down, preferred_element_type=jn...  4.27 us
    reshape x2, local copies, waits for them, and re-layouts, padded_path(): results.reshape(local_count, devices, MOST, features).transpose(1, 0, 2, 3)  3.36 us
    transpose x1, local copies, waits for them, and re-layouts, padded_path(): stacked = arrived.reshape(devices, local_count, MOST, features).transpose...  2.97 us
    dot_general x1, matrix products, run_experts(): jnp.einsum('erd,edf->erf', stacked, expert_gate, preferred_element_type=j...  2.92 us
    reshape x1, local copies, waits for them, and re-layouts, padded_path(): stacked = arrived.reshape(devices, local_count, MOST, features).transpose...  2.54 us
  transfers between devices with their start and end apart: 1, of which 1 were waited for; matrix products, arithmetic and copies ran while one was open for 1% of the time, Pallas kernels for 0%

commit v1 on v0

v1 whole, which is shorter than its diff:
```python
import jax
import jax.numpy as jnp
from jax import lax
from jax.experimental import pallas as pl
from jax.experimental.pallas import tpu as pltpu
from jax.sharding import PartitionSpec as P

MESH = pl.DeviceIdType.MESH
EPS = 1e-06
BF = jnp.bfloat16
F32 = jnp.float32
D = 1024
WIDE = 1152
CUT = 384
WIDTH = (384, 384, 256)
ORDER = (0, 1, 3, 2)


def kernel(
    lengths_ref, tokens_ref, routes_ref, gates_ref, ng_ref, og_ref,
    eg_ref, eu_ref, ed_ref, sg_ref, su_ref, sd_ref,
    out_ref,
    xg, yb, r1a, r1b, r1c, s1a, s1b, s1c, r2a, r2b, r2c, s2a, s2b, s2c, r3a, r3b, r3c,
    wg, wu, wd, sgv, suv, sdv, rows, meta_a, meta_b, hs, total,
    ag_send, ag_recv, rs_send, rs_recv, w_send, w_recv, w_local,
):
    me = lax.axis_index("ep")
    core = lax.rem(me, 2)
    chip = me // 2
    c = (chip // 16, lax.rem(chip // 4, 4), lax.rem(chip, 4))
    stride = (32, 8, 2)
    partner = me + 1 - 2 * core

    def shifted(dim, o):
        return lax.rem(c[dim] + o, 4)

    def device(dim, o):
        return me + (shifted(dim, o) - c[dim]) * stride[dim]

    barrier = pltpu.get_barrier_semaphore()
    pl.semaphore_signal(barrier, inc=1, device_id=(partner,), device_id_type=MESH)
    for dim in range(3):
        for o in (1, 2, 3):
            pl.semaphore_signal(
                barrier, inc=1, device_id=(device(dim, o),), device_id_type=MESH
            )

    mine = pl.ds(2 * core, 2)
    local = []
    for n, (src, dst) in enumerate(
        (
            (eg_ref, wg.at[mine]), (eu_ref, wu.at[mine]), (ed_ref, wd.at[mine]),
            (sg_ref, sgv), (su_ref, suv), (sd_ref, sdv),
        )
    ):
        copy = pltpu.make_async_copy(src, dst, w_local.at[n])
        copy.start()
        local.append(copy)

    row = lax.broadcasted_iota(jnp.int32, (16, 1), 0)
    limit = jnp.zeros((16, 1), jnp.int32)
    for s in range(4):
        limit = jnp.where(row // 4 == s, lengths_ref[s], limit)
        rows[4 * s : 4 * s + 4, :] = tokens_ref[s].astype(F32)
        meta_a[4 * s : 4 * s + 4, 0:8] = routes_ref[s].astype(F32)
        meta_b[4 * s : 4 * s + 4, 0:8] = gates_ref[s]
    live = lax.rem(row, 4) < limit
    values = rows[...]
    mean = jnp.mean(values * values, axis=-1, keepdims=True)
    normed = (values * lax.rsqrt(mean + EPS) * ng_ref[...]).astype(BF)
    lane = lax.broadcasted_iota(jnp.int32, (16, 128), 1)
    ids = jnp.where(live, meta_a[...], -1.0)
    gate = meta_b[...]
    high = gate.astype(BF).astype(F32)
    low = gate - high
    packed = jnp.where(
        lane < 8,
        ids,
        jnp.where(
            lane < 16,
            pltpu.roll(high, 8, 1),
            jnp.where(lane < 24, pltpu.roll(low, 16, 1), 0.0),
        ),
    )
    xg[c[0], c[1], c[2], :, 0:D] = normed
    xg[c[0], c[1], c[2], :, D:WIDE] = packed.astype(BF)

    pl.semaphore_wait(barrier, 10)

    def swap(n, dst_slot):
        src, dst = ((eg_ref, wg), (eu_ref, wu), (ed_ref, wd))[n]
        return pltpu.make_async_remote_copy(
            src_ref=src, dst_ref=dst.at[dst_slot], send_sem=w_send.at[n],
            recv_sem=w_recv.at[n], device_id=(partner,), device_id_type=MESH,
        )

    theirs = pl.ds(2 - 2 * core, 2)

    def ag(stage, part, o, sub=None, incoming=False):
        dim = (part + stage) % 3
        index = [c[0], c[1], c[2]]
        for t in range(stage):
            index[(part + t) % 3] = slice(None)
        if sub is not None:
            index[0] = lax.rem(c[0] + sub, 4)
        if incoming:
            index[dim] = shifted(dim, 4 - o)
        ref = xg.at[index[0], index[1], index[2], :, pl.ds(CUT * part, CUT)]
        if stage < 2:
            n = stage * 9 + part * 3 + o - 1
        elif part == 1:
            n = 42 + o - 1
        else:
            n = 18 + (12 if part == 2 else 0) + sub * 3 + o - 1
        return pltpu.make_async_remote_copy(
            src_ref=ref, dst_ref=ref, send_sem=ag_send.at[n], recv_sem=ag_recv.at[n],
            device_id=(device(dim, o),), device_id_type=MESH,
        )

    sent = []

    def go(copy):
        copy.start()
        sent.append(copy)

    for part in range(3):
        for o in (1, 3, 2):
            go(ag(0, part, o))
    for n in range(3):
        go(swap(n, mine))
    for part in range(3):
        for o in (1, 3, 2):
            ag(0, part, o, incoming=True).wait_recv()
        for o in (1, 3, 2):
            go(ag(1, part, o))
    for part in (1, 0, 2):
        for o in (1, 3, 2):
            ag(1, part, o, incoming=True).wait_recv()
        if part == 1:
            for o in (1, 3, 2):
                go(ag(2, 1, o))
        else:
            for sub in ORDER:
                for o in (1, 3, 2):
                    go(ag(2, part, o, sub=sub))

    for copy in local:
        copy.wait()
    own = xg[c[0], c[1], c[2], :, 0:D]
    part_g = jnp.dot(own, sgv[...], preferred_element_type=F32)
    part_u = jnp.dot(own, suv[...], preferred_element_type=F32)
    hidden = (part_g / (1.0 + jnp.exp(-part_g)) * part_u).astype(BF)
    total[...] = jnp.dot(hidden, sdv[...], preferred_element_type=F32)

    for n in range(3):
        swap(n, theirs).wait_recv()

    r1, s1 = (r1a, r1b, r1c), (s1a, s1b, s1c)
    r2, s2 = (r2a, r2b, r2c), (s2a, s2b, s2c)
    r3 = (r3a, r3b, r3c)

    def columns(part):
        return pl.ds(CUT * part, WIDTH[part])

    def rs1(part, o, sub=None):
        dim = (part + 2) % 3
        to = shifted(dim, o)
        k = None if sub is None else lax.rem(c[0] + sub, 4)
        if part == 0:
            src, dst = yb.at[k, :, to, :, columns(0)], r1a.at[o - 1, k]
            n = sub * 3 + o - 1
        elif part == 1:
            src, dst = yb.at[to, :, :, :, columns(1)], r1b.at[o - 1]
            n = 24 + o - 1
        else:
            src, dst = yb.at[k, to, :, :, columns(2)], r1c.at[o - 1, k]
            n = 12 + sub * 3 + o - 1
        return pltpu.make_async_remote_copy(
            src_ref=src, dst_ref=dst, send_sem=rs_send.at[n], recv_sem=rs_recv.at[n],
            device_id=(device(dim, o),), device_id_type=MESH,
        )

    def rs2(part, o):
        dim = (part + 1) % 3
        to = shifted(dim, o)
        src = s1[part].at[to] if part == 2 else s1[part].at[:, to]
        n = 27 + part * 3 + o - 1
        return pltpu.make_async_remote_copy(
            src_ref=src, dst_ref=r2[part].at[o - 1], send_sem=rs_send.at[n],
            recv_sem=rs_recv.at[n], device_id=(device(dim, o),), device_id_type=MESH,
        )

    def rs3(part, o):
        dim = part
        n = 36 + part * 3 + o - 1
        return pltpu.make_async_remote_copy(
            src_ref=s2[part].at[shifted(dim, o)], dst_ref=r3[part].at[o - 1],
            send_sem=rs_send.at[n], recv_sem=rs_recv.at[n],
            device_id=(device(dim, o),), device_id_type=MESH,
        )

    wide_lane = lax.broadcasted_iota(jnp.int32, (256, 128), 1)
    for off in ORDER:
        k = lax.rem(c[0] + off, 4)
        for o in (1, 3, 2):
            ag(2, 0, o, sub=off, incoming=True).wait_recv()
            ag(2, 2, o, sub=off, incoming=True).wait_recv()
        if off != 0:
            ag(2, 1, 4 - off, incoming=True).wait_recv()
        info = xg[k, :, :, :, D:WIDE].reshape(256, 128).astype(F32)
        weights = pltpu.roll(info, 120, 1) + pltpu.roll(info, 112, 1)
        x = xg[k, :, :, :, 0:D].reshape(256, D)
        for e in range(4):
            name = (4 * chip + e).astype(F32)
            hit = jnp.where((info == name) & (wide_lane < 8), weights, 0.0)
            w = jnp.sum(hit, axis=1, keepdims=True)
            g = jnp.dot(x, wg[e], preferred_element_type=F32)
            u = jnp.dot(x, wu[e], preferred_element_type=F32)
            hs[:, 256 * e : 256 * e + 256] = (g / (1.0 + jnp.exp(-g)) * u * w).astype(BF)
        y = jnp.dot(hs[...], wd[...].reshape(D, D), preferred_element_type=F32)
        yb[k] = y.astype(BF).reshape(4, 4, 16, D)
        for o in (1, 3, 2):
            go(rs1(0, o, sub=off))
            go(rs1(2, o, sub=off))
        if off != 0:
            go(rs1(1, off))

    for part in (0, 2, 1):
        for o in (1, 3, 2):
            if part == 1:
                rs1(1, o).wait_recv()
            else:
                for sub in ORDER:
                    rs1(part, o, sub=sub).wait_recv()
        if part == 0:
            base = yb[:, :, c[2], :, columns(0)]
        elif part == 1:
            base = yb[c[0], :, :, :, columns(1)]
        else:
            base = yb[:, c[1], :, :, columns(2)]
        acc = base.astype(F32)
        for o in (1, 2, 3):
            acc = acc + r1[part][o - 1].astype(F32)
        s1[part][...] = acc.astype(BF)
        for o in (1, 3, 2):
            go(rs2(part, o))
    for part in (0, 2, 1):
        for o in (1, 3, 2):
            rs2(part, o).wait_recv()
        dim = (part + 1) % 3
        base = s1[part][c[dim]] if part == 2 else s1[part][:, c[dim]]
        acc = base.astype(F32)
        for o in (1, 2, 3):
            acc = acc + r2[part][o - 1].astype(F32)
        s2[part][...] = acc.astype(BF)
        for o in (1, 3, 2):
            go(rs3(part, o))
    for part in (0, 2, 1):
        for o in (1, 3, 2):
            rs3(part, o).wait_recv()
        acc = s2[part][c[part]].astype(F32)
        for o in (1, 2, 3):
            acc = acc + r3[part][o - 1].astype(F32)
        total[:, CUT * part : CUT * part + WIDTH[part]] += acc

    summed = total[...]
    mean = jnp.mean(summed * summed, axis=-1, keepdims=True)
    mixed = jnp.where(live, summed * lax.rsqrt(mean + EPS) * og_ref[...], 0.0)
    mixed = mixed.astype(BF)
    for s in range(4):
        out_ref[s] = mixed[4 * s : 4 * s + 4, :]
    for copy in sent:
        copy.wait_send()


def per_device(
    tokens, lengths, routes, gates, norm_gain,
    expert_gate, expert_up, expert_down, shared_gate, shared_up, shared_down, out_gain,
):
    vmem = pl.BlockSpec(memory_space=pltpu.VMEM)
    hbm = pl.BlockSpec(memory_space=pl.ANY)
    dma = pltpu.SemaphoreType.DMA
    buffers = [pltpu.VMEM((4, 4, 4, 16, WIDE), BF), pltpu.VMEM((4, 4, 4, 16, D), BF)]
    buffers += [pltpu.VMEM((3, 4, 4, 16, w), BF) for w in WIDTH]
    buffers += [pltpu.VMEM((4, 4, 16, w), BF) for w in WIDTH]
    buffers += [pltpu.VMEM((3, 4, 16, w), BF) for w in WIDTH]
    buffers += [pltpu.VMEM((4, 16, w), BF) for w in WIDTH]
    buffers += [pltpu.VMEM((3, 16, w), BF) for w in WIDTH]
    buffers += [
        pltpu.VMEM((4, D, 256), BF), pltpu.VMEM((4, D, 256), BF), pltpu.VMEM((4, 256, D), BF),
        pltpu.VMEM((D, 256), BF), pltpu.VMEM((D, 256), BF), pltpu.VMEM((256, D), BF),
        pltpu.VMEM((16, D), F32), pltpu.VMEM((16, 128), F32), pltpu.VMEM((16, 128), F32),
        pltpu.VMEM((256, D), BF), pltpu.VMEM((16, D), F32),
    ]
    return pl.pallas_call(
        kernel,
        out_shape=jax.ShapeDtypeStruct(tokens.shape, BF),
        in_specs=[pl.BlockSpec(memory_space=pltpu.SMEM)] + [vmem] * 5 + [hbm] * 6,
        out_specs=vmem,
        scratch_shapes=buffers
        + [dma((45,)), dma((45,)), dma((45,)), dma((45,)), dma((3,)), dma((3,)), dma((6,))],
        compiler_params=pltpu.CompilerParams(
            collective_id=0, has_side_effects=True, vmem_limit_bytes=48 * 2**20
        ),
    )(
        lengths, tokens, routes, gates, norm_gain.reshape(1, D), out_gain.reshape(1, D),
        expert_gate, expert_up, expert_down, shared_gate, shared_up, shared_down,
    )


def solution(mesh):
    placed = (
        P("ep", None, None), P("ep"), P("ep", None, None), P("ep", None, None), P(),
        P("ep", None, None), P("ep", None, None), P("ep", None, None), P(), P(), P(), P(),
    )
    return jax.shard_map(
        per_device, mesh=mesh, in_specs=placed, out_specs=P("ep", None, None), check_vma=False
    )
```

time: 114 us -> 57.5 us (0.50)
  Pallas kernels: 0 us -> 45.3 us
  blocking collectives: 42.9 us -> 0 us
  waiting for transfers between devices: 32.5 us -> 0 us
  matrix products: 10.2 us -> 0 us
  local copies, waits for them, and re-layouts: 18 us -> 11.6 us
  starting transfers between devices: 4.78 us -> 0 us
  other arithmetic: 4.01 us -> 0 us
    pallas_call x0 -> x1, Pallas kernels: none -> 45.3 us  [per_device(): pl.pallas_call(kernel, out_shape=jax.ShapeDtypeStruct(tokens.shape, BF),...]
    all_to_all x1 -> x0, blocking collectives: 42.9 us -> none  [padded_path(): lax.all_to_all(outgoing, 'ep', split_axis=0, concat_axis=0, tiled=True)]
    all_to_all x1 -> x0, waiting for transfers between devices: 32.5 us -> none  [padded_path(): lax.all_to_all(replies, 'ep', split_axis=0, concat_axis=0, tiled=True)]
    unnamed x6 -> x25, local copies, waits for them, and re-layouts: 0.01 us -> 11.6 us
    dot_general x4 -> x0, matrix products: 10.2 us -> none  [the longest x1 4.27 us: run_experts(): jnp.einsum('erf,efd->erd', hidden, expert_down, preferred_element_type=jn...]
    reshape x6 -> x0, local copies, waits for them, and re-layouts: 9.14 us -> none  [the longest x2 3.36 us: padded_path(): results.reshape(local_count, devices, MOST, features).transpose(1, 0, 2, 3)]
    all_to_all x1 -> x0, starting transfers between devices: 4.78 us -> none  [padded_path(): lax.all_to_all(replies, 'ep', split_axis=0, concat_axis=0, tiled=True)]
    transpose x1 -> x0, local copies, waits for them, and re-layouts: 2.97 us -> none  [padded_path(): stacked = arrived.reshape(devices, local_count, MOST, features).transpose...]
  transfers between devices with their start and end apart: 1 -> 0, of which waited for: 1 -> 0; matrix products, arithmetic and copies ran while one was open for 1% -> 0% of each run, Pallas kernels for 0% -> 0%
where the time goes in v1:
time: 57.5 us; the launch traced here: 56.9 us
  Pallas kernels  45.3 us (79%)
  local copies, waits for them, and re-layouts  11.6 us (20%)
    pallas_call x1, Pallas kernels, per_device(): pl.pallas_call(kernel, out_shape=jax.ShapeDtypeStruct(tokens.shape, BF),...  45.3 us
    unnamed x25, local copies, waits for them, and re-layouts  11.6 us

profile of v1, /device:TPU:0, one launch (start us, length us, event | category | flops | bytes accessed | tf_op | source)
XLA Modules:
  0.0 56.9 jit_solution(15706787259098615265)
XLA Ops:
  0.0 0.0 copy-start.11
  0.0 0.7 %copy-done.11 = s32[4]{0:T(128)S(1)} copy-done((s32[4]{0:T(128)S(1)}, s32[4]{0:T(128)}, u32[]{:S(2)}) %copy-start.11) | copy-done | bytes 40
  0.7 0.0 copy-start
  0.7 1.2 %copy-done = bf16[2,1024,256]{2,1,0:T(8,128)(2,1)S(1)} copy-done((bf16[2,1024,256]{2,1,0:T(8,128)(2,1)S(1)}, bf16[2,1024,256]{2,1,0:T(8,128)(2,1)}, u32[]{:S(2)}) %copy-start) | copy-done | bytes 1048600
  1.9 0.0 copy-start.1
  1.9 1.2 %copy-done.1 = bf16[2,1024,256]{2,1,0:T(8,128)(2,1)S(1)} copy-done((bf16[2,1024,256]{2,1,0:T(8,128)(2,1)S(1)}, bf16[2,1024,256]{2,1,0:T(8,128)(2,1)}, u32[]{:S(2)}) %copy-start.1) | copy-done | bytes 1048600
  3.1 0.0 copy-start.2
  3.1 1.2 %copy-done.2 = bf16[2,256,1024]{2,1,0:T(8,128)(2,1)S(1)} copy-done((bf16[2,256,1024]{2,1,0:T(8,128)(2,1)S(1)}, bf16[2,256,1024]{2,1,0:T(8,128)(2,1)}, u32[]{:S(2)}) %copy-start.2) | copy-done | bytes 1048600
  4.3 0.0 copy-start.3
  4.3 1.0 %copy-done.3 = bf16[1024,256]{1,0:T(8,128)(2,1)S(1)} copy-done((bf16[1024,256]{1,0:T(8,128)(2,1)S(1)}, bf16[1024,256]{1,0:T(8,128)(2,1)}, u32[]{:S(2)}) %copy-start.3) | copy-done | bytes 524312
  5.4 0.0 copy-start.4
  5.4 1.0 %copy-done.4 = bf16[1024,256]{1,0:T(8,128)(2,1)S(1)} copy-done((bf16[1024,256]{1,0:T(8,128)(2,1)S(1)}, bf16[1024,256]{1,0:T(8,128)(2,1)}, u32[]{:S(2)}) %copy-start.4) | copy-done | bytes 524312
  6.4 0.0 copy-start.5
  6.4 1.0 %copy-done.5 = bf16[256,1024]{1,0:T(8,128)(2,1)S(1)} copy-done((bf16[256,1024]{1,0:T(8,128)(2,1)S(1)}, bf16[256,1024]{1,0:T(8,128)(2,1)}, u32[]{:S(2)}) %copy-start.5) | copy-done | bytes 524312
  7.5 0.0 copy-start.6
  7.5 0.8 %copy-done.6 = bf16[4,4,1024]{2,1,0:T(4,128)(2,1)S(1)} copy-done((bf16[4,4,1024]{2,1,0:T(4,128)(2,1)S(1)}, bf16[4,4,1024]{2,1,0:T(4,128)(2,1)}, u32[]{:S(2)}) %copy-start.6) | copy-done | bytes 32792
  8.2 0.0 copy-start.7
  8.2 0.7 %copy-done.7 = s32[4,4,8]{2,1,0:T(4,128)S(1)} copy-done((s32[4,4,8]{2,1,0:T(4,128)S(1)}, s32[4,4,8]{2,1,0:T(4,128)}, u32[]{:S(2)}) %copy-start.7) | copy-done | bytes 536
  8.9 0.0 copy-start.8
  8.9 0.7 %copy-done.8 = f32[4,4,8]{2,1,0:T(4,128)S(1)} copy-done((f32[4,4,8]{2,1,0:T(4,128)S(1)}, f32[4,4,8]{2,1,0:T(4,128)}, u32[]{:S(2)}) %copy-start.8) | copy-done | bytes 536
  9.6 0.7 %copy-done.9 = f32[1024]{0:T(1024)S(1)} copy-done((f32[1024]{0:T(1024)S(1)}, f32[1024]{0:T(1024)}, u32[]{:S(2)}) %copy-start.9) | copy-done | bytes 4120
  10.3 0.7 %copy-done.10 = f32[1024]{0:T(1024)S(1)} copy-done((f32[1024]{0:T(1024)S(1)}, f32[1024]{0:T(1024)}, u32[]{:S(2)}) %copy-start.10) | copy-done | bytes 4120
  11.0 45.3 %shard_map.118 = bf16[4,4,1024]{2,1,0:T(4,128)(2,1)S(1)} custom-call(s32[4]{0:T(128)S(1)} %copy-done.11, bf16[4,4,1024]{2,1,0:T(4,128)(2,1)S(1)} %copy-done.6, s32[4,4,8]{2,1,0:T(4,128)S(1)} %copy-done.7, f32[4,4,8]{2,1,0:T(4,128)S(1)} %copy-done.8, f32[1,1024]{1,0:T(1,128)S(1)} %bitcast.2, f32[1,1024]{1,0:T(1,128)S(1)} %bitcast.3, ...), custom_call_target="tpu_custom_call" | custom-call | tf_op jit(solution)/shard_map/pallas_call | solution.py:295
  56.3 0.6 %copy.14 = bf16[4,4,1024]{2,1,0:T(4,128)(2,1)} copy(bf16[4,4,1024]{2,1,0:T(4,128)(2,1)S(1)} %shard_map.118) | data formatting | bytes 65536
  (2 shorter events, 0.0 us)
Async XLA Ops:
  0.0 0.7 %copy-start.11 = (s32[4]{0:T(128)S(1)}, s32[4]{0:T(128)}, u32[]{:S(2)}) copy-start(s32[4]{0:T(128)} %lengths_ref.1) | copy-start | bytes 52
  0.7 1.2 %copy-start = (bf16[2,1024,256]{2,1,0:T(8,128)(2,1)S(1)}, bf16[2,1024,256]{2,1,0:T(8,128)(2,1)}, u32[]{:S(2)}) copy-start(bf16[2,1024,256]{2,1,0:T(8,128)(2,1)} %eg_ref.1) | copy-start | bytes 3145732
  1.9 1.2 %copy-start.1 = (bf16[2,1024,256]{2,1,0:T(8,128)(2,1)S(1)}, bf16[2,1024,256]{2,1,0:T(8,128)(2,1)}, u32[]{:S(2)}) copy-start(bf16[2,1024,256]{2,1,0:T(8,128)(2,1)} %eu_ref.1) | copy-start | bytes 3145732
  3.1 1.2 %copy-start.2 = (bf16[2,256,1024]{2,1,0:T(8,128)(2,1)S(1)}, bf16[2,256,1024]{2,1,0:T(8,128)(2,1)}, u32[]{:S(2)}) copy-start(bf16[2,256,1024]{2,1,0:T(8,128)(2,1)} %ed_ref.1) | copy-start | bytes 3145732
  4.3 1.0 %copy-start.3 = (bf16[1024,256]{1,0:T(8,128)(2,1)S(1)}, bf16[1024,256]{1,0:T(8,128)(2,1)}, u32[]{:S(2)}) copy-start(bf16[1024,256]{1,0:T(8,128)(2,1)} %sg_ref.1) | copy-start | bytes 1572868
  5.4 1.0 %copy-start.4 = (bf16[1024,256]{1,0:T(8,128)(2,1)S(1)}, bf16[1024,256]{1,0:T(8,128)(2,1)}, u32[]{:S(2)}) copy-start(bf16[1024,256]{1,0:T(8,128)(2,1)} %su_ref.1) | copy-start | bytes 1572868
  6.4 1.0 %copy-start.5 = (bf16[256,1024]{1,0:T(8,128)(2,1)S(1)}, bf16[256,1024]{1,0:T(8,128)(2,1)}, u32[]{:S(2)}) copy-start(bf16[256,1024]{1,0:T(8,128)(2,1)} %sd_ref.1) | copy-start | bytes 1572868
  7.5 0.8 %copy-start.6 = (bf16[4,4,1024]{2,1,0:T(4,128)(2,1)S(1)}, bf16[4,4,1024]{2,1,0:T(4,128)(2,1)}, u32[]{:S(2)}) copy-start(bf16[4,4,1024]{2,1,0:T(4,128)(2,1)} %tokens_ref.1) | copy-start | bytes 98308
  8.2 0.7 %copy-start.7 = (s32[4,4,8]{2,1,0:T(4,128)S(1)}, s32[4,4,8]{2,1,0:T(4,128)}, u32[]{:S(2)}) copy-start(s32[4,4,8]{2,1,0:T(4,128)} %routes_ref.1) | copy-start | bytes 1540
  8.9 0.7 %copy-start.8 = (f32[4,4,8]{2,1,0:T(4,128)S(1)}, f32[4,4,8]{2,1,0:T(4,128)}, u32[]{:S(2)}) copy-start(f32[4,4,8]{2,1,0:T(4,128)} %gates_ref.1) | copy-start | bytes 1540
  9.6 0.7 %copy-start.9 = (f32[1024]{0:T(1024)S(1)}, f32[1024]{0:T(1024)}, u32[]{:S(2)}) copy-start(f32[1024]{0:T(1024)} %param.16) | copy-start | bytes 12292
  10.3 0.7 %copy-start.10 = (f32[1024]{0:T(1024)S(1)}, f32[1024]{0:T(1024)}, u32[]{:S(2)}) copy-start(f32[1024]{0:T(1024)} %param.23) | copy-start | bytes 12292

commit v2 on v1

--- a/solution.py
+++ b/solution.py
@@ -17,12 +17,13 @@
 
 
 def kernel(
-    lengths_ref, tokens_ref, routes_ref, gates_ref, ng_ref, og_ref,
+    lengths_hbm, tokens_hbm, routes_hbm, gates_hbm, ng_hbm, og_hbm,
     eg_ref, eu_ref, ed_ref, sg_ref, su_ref, sd_ref,
     out_ref,
     xg, yb, r1a, r1b, r1c, s1a, s1b, s1c, r2a, r2b, r2c, s2a, s2b, s2c, r3a, r3b, r3c,
     wg, wu, wd, sgv, suv, sdv, rows, meta_a, meta_b, hs, total,
-    ag_send, ag_recv, rs_send, rs_recv, w_send, w_recv, w_local,
+    lengths_ref, tokens_ref, routes_ref, gates_ref, ng_ref, og_ref,
+    ag_send, ag_recv, rs_send, rs_recv, w_send, w_recv, w_local, small,
 ):
     me = lax.axis_index("ep")
     core = lax.rem(me, 2)
@@ -45,6 +46,16 @@
                 barrier, inc=1, device_id=(device(dim, o),), device_id_type=MESH
             )
 
+    early = []
+    for n, (src, dst) in enumerate(
+        (
+            (tokens_hbm, tokens_ref), (ng_hbm, ng_ref), (routes_hbm, routes_ref),
+            (gates_hbm, gates_ref), (lengths_hbm, lengths_ref), (og_hbm, og_ref),
+        )
+    ):
+        copy = pltpu.make_async_copy(src, dst, small.at[n])
+        copy.start()
+        early.append(copy)
     mine = pl.ds(2 * core, 2)
     local = []
     for n, (src, dst) in enumerate(
@@ -57,6 +68,8 @@
         copy.start()
         local.append(copy)
 
+    for copy in early:
+        copy.wait()
     row = lax.broadcasted_iota(jnp.int32, (16, 1), 0)
     limit = jnp.zeros((16, 1), jnp.int32)
     for s in range(4):
@@ -278,7 +291,7 @@
     expert_gate, expert_up, expert_down, shared_gate, shared_up, shared_down, out_gain,
 ):
     vmem = pl.BlockSpec(memory_space=pltpu.VMEM)
-    hbm = pl.BlockSpec(memory_space=pl.ANY)
+    hbm = pl.BlockSpec(memory_space=pltpu.HBM)
     dma = pltpu.SemaphoreType.DMA
     buffers = [pltpu.VMEM((4, 4, 4, 16, WIDE), BF), pltpu.VMEM((4, 4, 4, 16, D), BF)]
     buffers += [pltpu.VMEM((3, 4, 4, 16, w), BF) for w in WIDTH]
@@ -291,16 +304,19 @@
         pltpu.VMEM((D, 256), BF), pltpu.VMEM((D, 256), BF), pltpu.VMEM((256, D), BF),
         pltpu.VMEM((16, D), F32), pltpu.VMEM((16, 128), F32), pltpu.VMEM((16, 128), F32),
         pltpu.VMEM((256, D), BF), pltpu.VMEM((16, D), F32),
+        pltpu.SMEM((4,), jnp.int32), pltpu.VMEM((4, 4, D), BF),
+        pltpu.VMEM((4, 4, 8), jnp.int32), pltpu.VMEM((4, 4, 8), F32),
+        pltpu.VMEM((1, D), F32), pltpu.VMEM((1, D), F32),
     ]
     return pl.pallas_call(
         kernel,
         out_shape=jax.ShapeDtypeStruct(tokens.shape, BF),
-        in_specs=[pl.BlockSpec(memory_space=pltpu.SMEM)] + [vmem] * 5 + [hbm] * 6,
+        in_specs=[hbm] * 12,
         out_specs=vmem,
         scratch_shapes=buffers
-        + [dma((45,)), dma((45,)), dma((45,)), dma((45,)), dma((3,)), dma((3,)), dma((6,))],
+        + [dma((45,)), dma((45,)), dma((45,)), dma((45,)), dma((3,)), dma((3,)), dma((6,)), dma((6,))],
         compiler_params=pltpu.CompilerParams(
-            collective_id=0, has_side_effects=True, vmem_limit_bytes=48 * 2**20
+            collective_id=0, has_side_effects=True, vmem_limit_bytes=67043328
         ),
     )(
         lengths, tokens, routes, gates, norm_gain.reshape(1, D), out_gain.reshape(1, D),

time: 57.5 us -> 46.9 us (0.82)
  local copies, waits for them, and re-layouts: 11.6 us -> 1.39 us
    unnamed x25 -> x1, local copies, waits for them, and re-layouts: 11.6 us -> 1.39 us
where the time goes in v2:
time: 46.9 us; the launch traced here: 46.8 us
  Pallas kernels  45.4 us (97%)
  local copies, waits for them, and re-layouts  1.39 us (3%)
    pallas_call x1, Pallas kernels, per_device(): pl.pallas_call(kernel, out_shape=jax.ShapeDtypeStruct(tokens.shape, BF),...  45.4 us
    unnamed x1, local copies, waits for them, and re-layouts  1.39 us

profile of v2, /device:TPU:0, one launch (start us, length us, event | category | flops | bytes accessed | tf_op | source)
XLA Modules:
  0.0 46.8 jit_solution(13242395802528962058)
XLA Ops:
  0.0 45.4 %shard_map.118 = bf16[4,4,1024]{2,1,0:T(4,128)(2,1)} custom-call(s32[4]{0:T(128)} %lengths_hbm.1, bf16[4,4,1024]{2,1,0:T(4,128)(2,1)} %tokens_hbm.1, s32[4,4,8]{2,1,0:T(4,128)} %routes_hbm.1, f32[4,4,8]{2,1,0:T(4,128)} %gates_hbm.1, f32[1,1024]{1,0:T(1,128)} %bitcast.2, f32[1,1024]{1,0:T(1,128)} %bitcast.3, bf16[2,1024,256]{2,1,0:T(8,128)(2,1)} %eg_ref.1, ...), custom_call_target="tpu_custom_call" | custom-call | tf_op jit(solution)/shard_map/pallas_call | solution.py:311
  45.4 1.4 %copy.14 = bf16[4,4,1024]{2,1,0:T(4,128)(2,1)} copy(bf16[4,4,1024]{2,1,0:T(4,128)(2,1)} %shard_map.118) | data formatting | bytes 65536

commit v3 on v2

v3 whole, which is shorter than its diff:
```python
import jax
import jax.numpy as jnp
from jax import lax
from jax.experimental import pallas as pl
from jax.experimental.pallas import tpu as pltpu
from jax.sharding import PartitionSpec as P

MESH = pl.DeviceIdType.MESH
EPS = 1e-06
BF = jnp.bfloat16
F32 = jnp.float32
D = 1024
WIDE = 1152
CUT = 384
WIDTH = (384, 384, 256)
ORDER = (0, 1, 3, 2)
REST = slice(1, 4)
ALL = slice(None)


def kernel(
    lengths_hbm, tokens_hbm, routes_hbm, gates_hbm, ng_hbm, og_hbm,
    eg_ref, eu_ref, ed_ref, sg_ref, su_ref, sd_ref,
    out_ref,
    xg, yb, r1a, r1b, r1c, s1a, s1b, s1c, r2a, r2b, r2c, s2a, s2b, s2c, r3a, r3b, r3c,
    wg, wu, wd, sgv, suv, sdv, rows, meta_a, meta_b, hs, total,
    lengths_ref, tokens_ref, routes_ref, gates_ref, ng_ref, og_ref,
    send_sem, recv_sem, w_send, w_recv, w_local, small,
):
    me = lax.axis_index("ep")
    core = lax.rem(me, 2)
    chip = me // 2
    c = (chip // 16, lax.rem(chip // 4, 4), lax.rem(chip, 4))
    stride = (32, 8, 2)
    partner = me + 1 - 2 * core

    peers = [
        [me + (lax.rem(c[dim] + o, 4) - c[dim]) * stride[dim] for o in range(4)]
        for dim in range(3)
    ]

    barrier = pltpu.get_barrier_semaphore()
    pl.semaphore_signal(barrier, inc=1, device_id=(partner,), device_id_type=MESH)
    for dim in range(3):
        for o in (1, 2, 3):
            pl.semaphore_signal(
                barrier, inc=1, device_id=(peers[dim][o],), device_id_type=MESH
            )

    early = []
    for n, (src, dst) in enumerate(
        (
            (tokens_hbm, tokens_ref), (ng_hbm, ng_ref), (routes_hbm, routes_ref),
            (gates_hbm, gates_ref), (lengths_hbm, lengths_ref), (og_hbm, og_ref),
        )
    ):
        copy = pltpu.make_async_copy(src, dst, small.at[n])
        copy.start()
        early.append(copy)
    mine = pl.ds(2 * core, 2)
    local = []
    for n, (src, dst) in enumerate(
        (
            (eg_ref, wg.at[mine]), (eu_ref, wu.at[mine]), (ed_ref, wd.at[mine]),
            (sg_ref, sgv), (su_ref, suv), (sd_ref, sdv),
        )
    ):
        copy = pltpu.make_async_copy(src, dst, w_local.at[n])
        copy.start()
        local.append(copy)

    for copy in early:
        copy.wait()
    row = lax.broadcasted_iota(jnp.int32, (16, 1), 0)
    limit = jnp.zeros((16, 1), jnp.int32)
    for s in range(4):
        limit = jnp.where(row // 4 == s, lengths_ref[s], limit)
        rows[4 * s : 4 * s + 4, :] = tokens_ref[s].astype(F32)
        meta_a[4 * s : 4 * s + 4, 0:8] = routes_ref[s].astype(F32)
        meta_b[4 * s : 4 * s + 4, 0:8] = gates_ref[s]
    live = lax.rem(row, 4) < limit
    values = rows[...]
    mean = jnp.mean(values * values, axis=-1, keepdims=True)
    normed = (values * lax.rsqrt(mean + EPS) * ng_ref[...]).astype(BF)
    lane = lax.broadcasted_iota(jnp.int32, (16, 128), 1)
    ids = jnp.where(live, meta_a[...], -1.0)
    gate = meta_b[...]
    high = gate.astype(BF).astype(F32)
    low = gate - high
    packed = jnp.where(
        lane < 8,
        ids,
        jnp.where(
            lane < 16,
            pltpu.roll(high, 8, 1),
            jnp.where(lane < 24, pltpu.roll(low, 16, 1), 0.0),
        ),
    )
    xg[0, 0, 0, :, 0:D] = normed
    xg[0, 0, 0, :, D:WIDE] = packed.astype(BF)

    pl.semaphore_wait(barrier, 10)

    def swap(n, dst_slot):
        src, dst = ((eg_ref, wg), (eu_ref, wu), (ed_ref, wd))[n]
        return pltpu.make_async_remote_copy(
            src_ref=src, dst_ref=dst.at[dst_slot], send_sem=w_send.at[n],
            recv_sem=w_recv.at[n], device_id=(partner,), device_id_type=MESH,
        )

    theirs = pl.ds(2 - 2 * core, 2)

    copies = {}

    def block(ref, part, i, j, k, width=CUT):
        index = [0, 0, 0]
        index[part], index[(part + 1) % 3], index[(part + 2) % 3] = i, j, k
        return ref.at[index[0], index[1], index[2], :, pl.ds(CUT * part, width)]

    def send(key, src, dst, dim, o):
        n = len(copies)
        copies[key] = pltpu.make_async_remote_copy(
            src_ref=src, dst_ref=dst, send_sem=send_sem.at[n], recv_sem=recv_sem.at[n],
            device_id=(peers[dim % 3][o],), device_id_type=MESH,
        )
        copies[key].start()

    def arrive(*key):
        copies[key].wait_recv()

    near = (1, 3, 2)
    for part in range(3):
        for o in near:
            send(("a0", part, o), block(xg, part, 0, 0, 0), block(xg, part, 4 - o, 0, 0), part, o)
    for part in range(3):
        for o in near:
            send(
                ("a1o", part, o), block(xg, part, 0, 0, 0), block(xg, part, 0, 4 - o, 0), part + 1, o
            )
    for n in range(3):
        swap(n, mine).start()
    for part in range(3):
        for o in near:
            arrive("a0", part, o)
        for o in near:
            send(
                ("a1", part, o), block(xg, part, REST, 0, 0), block(xg, part, REST, 4 - o, 0), part + 1, o
            )
    for part in range(3):
        for o in near:
            send(
                ("a2l", part, o), block(xg, part, ALL, 0, 0), block(xg, part, ALL, 0, 4 - o), part + 2, o
            )
    for q in near:
        arrive("a1o", 2, 4 - q)
        arrive("a1", 2, 4 - q)
        for o in near:
            send(
                ("a2", 2, q, o), block(xg, 2, ALL, q, 0), block(xg, 2, ALL, q, 4 - o), 1, o
            )
    for o in near:
        arrive("a1o", 1, o)
        arrive("a1", 1, o)
    for o in near:
        send(("a2", 1, o), block(xg, 1, ALL, REST, 0), block(xg, 1, ALL, REST, 4 - o), 0, o)
    for o in near:
        arrive("a1o", 0, o)
        arrive("a1", 0, o)
    for k in ORDER:
        for o in near:
            send(("a2", 0, k, o), block(xg, 0, k, REST, 0), block(xg, 0, k, REST, 4 - o), 2, o)

    for copy in local:
        copy.wait()
    own = xg[0, 0, 0, :, 0:D]
    part_g = jnp.dot(own, sgv[...], preferred_element_type=F32)
    part_u = jnp.dot(own, suv[...], preferred_element_type=F32)
    hidden = (part_g / (1.0 + jnp.exp(-part_g)) * part_u).astype(BF)
    total[...] = jnp.dot(hidden, sdv[...], preferred_element_type=F32)

    for n in range(3):
        swap(n, theirs).wait_recv()

    r1, s1 = (r1a, r1b, r1c), (s1a, s1b, s1c)
    r2, s2 = (r2a, r2b, r2c), (s2a, s2b, s2c)
    r3 = (r3a, r3b, r3c)

    def out_block(part, i, j, k):
        return block(yb, part, i, j, k, WIDTH[part])

    wide_lane = lax.broadcasted_iota(jnp.int32, (256, 128), 1)
    for k in ORDER:
        if k == 0:
            for o in near:
                arrive("a2l", 0, o)
                arrive("a2l", 2, o)
        else:
            arrive("a2l", 1, 4 - k)
            arrive("a2", 1, 4 - k)
        for o in near:
            arrive("a2", 0, k, o)
            if k != 0:
                arrive("a2", 2, k, o)
        info = xg[k, :, :, :, D:WIDE].reshape(256, 128).astype(F32)
        weights = pltpu.roll(info, 120, 1) + pltpu.roll(info, 112, 1)
        x = xg[k, :, :, :, 0:D].reshape(256, D)
        for e in range(4):
            name = (4 * chip + e).astype(F32)
            hit = jnp.where((info == name) & (wide_lane < 8), weights, 0.0)
            w = jnp.sum(hit, axis=1, keepdims=True)
            g = jnp.dot(x, wg[e], preferred_element_type=F32)
            u = jnp.dot(x, wu[e], preferred_element_type=F32)
            hs[:, 256 * e : 256 * e + 256] = (g / (1.0 + jnp.exp(-g)) * u * w).astype(BF)
        y = jnp.dot(hs[...], wd[...].reshape(D, D), preferred_element_type=F32)
        yb[k] = y.astype(BF).reshape(4, 4, 16, D)
        for o in near:
            send(("r1", 0, k, o), out_block(0, k, REST, o), r1a.at[o - 1, k, REST], 2, o)
            if k != 0:
                send(("r1", 2, k, o), out_block(2, ALL, k, o), r1c.at[o - 1, k], 1, o)
        if k != 0:
            send(("r1", 1, k), out_block(1, ALL, REST, k), r1b.at[k - 1, :, REST], 0, k)
    for o in near:
        send(("r1l", 0, o), out_block(0, ALL, 0, o), r1a.at[o - 1, :, 0], 2, o)
        send(("r1l", 1, o), out_block(1, ALL, 0, o), r1b.at[o - 1, :, 0], 0, o)
        send(("r1l", 2, o), out_block(2, ALL, 0, o), r1c.at[o - 1, 0], 1, o)

    for k in (1, 3, 2):
        for o in near:
            arrive("r1", 2, k, o)
        acc = yb[k, 0, :, :, 2 * CUT : D].astype(F32)
        for o in (1, 2, 3):
            acc = acc + r1c[o - 1, k].astype(F32)
        s1c[k] = acc.astype(BF)
        send(("r2", 2, k), s1c.at[k, REST], r2c.at[k - 1, REST], 0, k)
    for o in near:
        arrive("r1", 1, o)
    acc = yb[0, :, 1:4, :, CUT : 2 * CUT].astype(F32)
    for o in (1, 2, 3):
        acc = acc + r1b[o - 1, :, 1:4].astype(F32)
    s1b[:, 1:4] = acc.astype(BF)
    for o in near:
        send(("r2", 1, o), s1b.at[REST, o], r2b.at[o - 1, REST], 2, o)
    for o in near:
        for k in ORDER:
            arrive("r1", 0, k, o)
    acc = yb[:, 1:4, 0, :, 0:CUT].astype(F32)
    for o in (1, 2, 3):
        acc = acc + r1a[o - 1, :, 1:4].astype(F32)
    s1a[:, 1:4] = acc.astype(BF)
    for o in near:
        send(("r2", 0, o), s1a.at[REST, o], r2a.at[o - 1, REST], 1, o)
    for o in near:
        send(("r2l", 2, o), s1c.at[o, 0], r2c.at[o - 1, 0], 0, o)
        send(("r2l", 1, o), s1b.at[0, o], r2b.at[o - 1, 0], 2, o)
        send(("r2l", 0, o), s1a.at[0, o], r2a.at[o - 1, 0], 1, o)

    for part in (2, 1, 0):
        for o in near:
            arrive("r1l", part, o)
        if part == 0:
            acc = yb[:, 0, 0, :, 0:CUT].astype(F32)
        elif part == 1:
            acc = yb[0, :, 0, :, CUT : 2 * CUT].astype(F32)
        else:
            acc = yb[0, 0, :, :, 2 * CUT : D].astype(F32)
        for o in (1, 2, 3):
            line = r1c[o - 1, 0] if part == 2 else r1[part][o - 1, :, 0]
            acc = acc + line.astype(F32)
        total[:, CUT * part : CUT * part + WIDTH[part]] += acc[0]
        for o in near:
            arrive("r2", part, o)
        acc = acc[1:4]
        for o in (1, 2, 3):
            acc = acc + r2[part][o - 1, 1:4].astype(F32)
        s2[part][1:4] = acc.astype(BF)
        for o in near:
            send(("r3", part, o), s2[part].at[o], r3[part].at[o - 1], part, o)
    for part in (2, 1, 0):
        for o in near:
            arrive("r2l", part, o)
        acc = r2[part][0, 0].astype(F32)
        for o in (2, 3):
            acc = acc + r2[part][o - 1, 0].astype(F32)
        for o in near:
            arrive("r3", part, o)
        for o in (1, 2, 3):
            acc = acc + r3[part][o - 1].astype(F32)
        total[:, CUT * part : CUT * part + WIDTH[part]] += acc

    summed = total[...]
    mean = jnp.mean(summed * summed, axis=-1, keepdims=True)
    mixed = jnp.where(live, summed * lax.rsqrt(mean + EPS) * og_ref[...], 0.0)
    mixed = mixed.astype(BF)
    for s in range(4):
        out_ref[s] = mixed[4 * s : 4 * s + 4, :]
    for copy in copies.values():
        copy.wait_send()
    for n in range(3):
        swap(n, mine).wait_send()


def per_device(
    tokens, lengths, routes, gates, norm_gain,
    expert_gate, expert_up, expert_down, shared_gate, shared_up, shared_down, out_gain,
):
    vmem = pl.BlockSpec(memory_space=pltpu.VMEM)
    hbm = pl.BlockSpec(memory_space=pltpu.HBM)
    dma = pltpu.SemaphoreType.DMA
    buffers = [pltpu.VMEM((4, 4, 4, 16, WIDE), BF), pltpu.VMEM((4, 4, 4, 16, D), BF)]
    buffers += [pltpu.VMEM((3, 4, 4, 16, w), BF) for w in WIDTH]
    buffers += [pltpu.VMEM((4, 4, 16, w), BF) for w in WIDTH]
    buffers += [pltpu.VMEM((3, 4, 16, w), BF) for w in WIDTH]
    buffers += [pltpu.VMEM((4, 16, w), BF) for w in WIDTH]
    buffers += [pltpu.VMEM((3, 16, w), BF) for w in WIDTH]
    buffers += [
        pltpu.VMEM((4, D, 256), BF), pltpu.VMEM((4, D, 256), BF), pltpu.VMEM((4, 256, D), BF),
        pltpu.VMEM((D, 256), BF), pltpu.VMEM((D, 256), BF), pltpu.VMEM((256, D), BF),
        pltpu.VMEM((16, D), F32), pltpu.VMEM((16, 128), F32), pltpu.VMEM((16, 128), F32),
        pltpu.VMEM((256, D), BF), pltpu.VMEM((16, D), F32),
        pltpu.SMEM((4,), jnp.int32), pltpu.VMEM((4, 4, D), BF),
        pltpu.VMEM((4, 4, 8), jnp.int32), pltpu.VMEM((4, 4, 8), F32),
        pltpu.VMEM((1, D), F32), pltpu.VMEM((1, D), F32),
    ]
    return pl.pallas_call(
        kernel,
        out_shape=jax.ShapeDtypeStruct(tokens.shape, BF),
        in_specs=[hbm] * 12,
        out_specs=vmem,
        scratch_shapes=buffers
        + [dma((120,)), dma((120,)), dma((3,)), dma((3,)), dma((6,)), dma((6,))],
        compiler_params=pltpu.CompilerParams(
            collective_id=0, has_side_effects=True, vmem_limit_bytes=67043328
        ),
    )(
        lengths, tokens, routes, gates, norm_gain.reshape(1, D), out_gain.reshape(1, D),
        expert_gate, expert_up, expert_down, shared_gate, shared_up, shared_down,
    )


def solution(mesh):
    placed = (
        P("ep", None, None), P("ep"), P("ep", None, None), P("ep", None, None), P(),
        P("ep", None, None), P("ep", None, None), P("ep", None, None), P(), P(), P(), P(),
    )
    return jax.shard_map(
        per_device, mesh=mesh, in_specs=placed, out_specs=P("ep", None, None), check_vma=False
    )
```

time: 46.9 us -> 46.2 us (0.985)
  Pallas kernels: 45.4 us -> 44.6 us
    pallas_call x1, Pallas kernels: 45.4 us -> 44.6 us  [per_device(): pl.pallas_call(kernel, out_shape=jax.ShapeDtypeStruct(tokens.shape, BF),...]
where the time goes in v3:
time: 46.2 us; the launch traced here: 46 us
  Pallas kernels  44.6 us (97%)
  local copies, waits for them, and re-layouts  1.39 us (3%)
    pallas_call x1, Pallas kernels, per_device(): pl.pallas_call(kernel, out_shape=jax.ShapeDtypeStruct(tokens.shape, BF),...  44.6 us
    unnamed x1, local copies, waits for them, and re-layouts  1.39 us

profile of v3, /device:TPU:0, one launch (start us, length us, event | category | flops | bytes accessed | tf_op | source)
XLA Modules:
  0.0 46.0 jit_solution(8213404574659398537)
XLA Ops:
  0.0 44.6 %shard_map.118 = bf16[4,4,1024]{2,1,0:T(4,128)(2,1)} custom-call(s32[4]{0:T(128)} %lengths_hbm.1, bf16[4,4,1024]{2,1,0:T(4,128)(2,1)} %tokens_hbm.1, s32[4,4,8]{2,1,0:T(4,128)} %routes_hbm.1, f32[4,4,8]{2,1,0:T(4,128)} %gates_hbm.1, f32[1,1024]{1,0:T(1,128)} %bitcast.2, f32[1,1024]{1,0:T(1,128)} %bitcast.3, bf16[2,1024,256]{2,1,0:T(8,128)(2,1)} %eg_ref.1, ...), custom_call_target="tpu_custom_call" | custom-call | tf_op jit(solution)/shard_map/pallas_call | solution.py:324
  44.6 1.4 %copy.14 = bf16[4,4,1024]{2,1,0:T(4,128)(2,1)} copy(bf16[4,4,1024]{2,1,0:T(4,128)(2,1)} %shard_map.118) | data formatting | bytes 65536

commit v4 on v3

--- a/solution.py
+++ b/solution.py
@@ -151,24 +151,22 @@
             send(
                 ("a2l", part, o), block(xg, part, ALL, 0, 0), block(xg, part, ALL, 0, 4 - o), part + 2, o
             )
+    for o in near:
+        arrive("a1o", 0, o)
+        arrive("a1", 0, o)
+    for k in ORDER:
+        for o in near:
+            send(("a2", 0, k, o), block(xg, 0, k, REST, 0), block(xg, 0, k, REST, 4 - o), 2, o)
+    for o in near:
+        arrive("a1o", 1, o)
+        arrive("a1", 1, o)
+    for o in near:
+        send(("a2", 1, o), block(xg, 1, ALL, REST, 0), block(xg, 1, ALL, REST, 4 - o), 0, o)
     for q in near:
         arrive("a1o", 2, 4 - q)
         arrive("a1", 2, 4 - q)
         for o in near:
-            send(
-                ("a2", 2, q, o), block(xg, 2, ALL, q, 0), block(xg, 2, ALL, q, 4 - o), 1, o
-            )
-    for o in near:
-        arrive("a1o", 1, o)
-        arrive("a1", 1, o)
-    for o in near:
-        send(("a2", 1, o), block(xg, 1, ALL, REST, 0), block(xg, 1, ALL, REST, 4 - o), 0, o)
-    for o in near:
-        arrive("a1o", 0, o)
-        arrive("a1", 0, o)
-    for k in ORDER:
-        for o in near:
-            send(("a2", 0, k, o), block(xg, 0, k, REST, 0), block(xg, 0, k, REST, 4 - o), 2, o)
+            send(("a2", 2, q, o), block(xg, 2, ALL, q, 0), block(xg, 2, ALL, q, 4 - o), 1, o)
 
     for copy in local:
         copy.wait()

time: 46.2 us -> 45.8 us (level)
  no operation moved by 1% of the time
where the time goes in v4:
time: 45.8 us; the launch traced here: 45.6 us
  Pallas kernels  44.3 us (97%)
  local copies, waits for them, and re-layouts  1.39 us (3%)
    pallas_call x1, Pallas kernels, per_device(): pl.pallas_call(kernel, out_shape=jax.ShapeDtypeStruct(tokens.shape, BF),...  44.3 us
    unnamed x1, local copies, waits for them, and re-layouts  1.39 us

profile of v4, /device:TPU:0, one launch (start us, length us, event | category | flops | bytes accessed | tf_op | source)
XLA Modules:
  0.0 45.6 jit_solution(15176475601787667829)
XLA Ops:
  0.0 44.3 %shard_map.118 = bf16[4,4,1024]{2,1,0:T(4,128)(2,1)} custom-call(s32[4]{0:T(128)} %lengths_hbm.1, bf16[4,4,1024]{2,1,0:T(4,128)(2,1)} %tokens_hbm.1, s32[4,4,8]{2,1,0:T(4,128)} %routes_hbm.1, f32[4,4,8]{2,1,0:T(4,128)} %gates_hbm.1, f32[1,1024]{1,0:T(1,128)} %bitcast.2, f32[1,1024]{1,0:T(1,128)} %bitcast.3, bf16[2,1024,256]{2,1,0:T(8,128)(2,1)} %eg_ref.1, ...), custom_call_target="tpu_custom_call" | custom-call | tf_op jit(solution)/shard_map/pallas_call | solution.py:322
  44.3 1.4 %copy.14 = bf16[4,4,1024]{2,1,0:T(4,128)(2,1)} copy(bf16[4,4,1024]{2,1,0:T(4,128)(2,1)} %shard_map.118) | data formatting | bytes 65536

commit v5 on v4

--- a/solution.py
+++ b/solution.py
@@ -82,22 +82,7 @@
     values = rows[...]
     mean = jnp.mean(values * values, axis=-1, keepdims=True)
     normed = (values * lax.rsqrt(mean + EPS) * ng_ref[...]).astype(BF)
-    lane = lax.broadcasted_iota(jnp.int32, (16, 128), 1)
-    ids = jnp.where(live, meta_a[...], -1.0)
-    gate = meta_b[...]
-    high = gate.astype(BF).astype(F32)
-    low = gate - high
-    packed = jnp.where(
-        lane < 8,
-        ids,
-        jnp.where(
-            lane < 16,
-            pltpu.roll(high, 8, 1),
-            jnp.where(lane < 24, pltpu.roll(low, 16, 1), 0.0),
-        ),
-    )
     xg[0, 0, 0, :, 0:D] = normed
-    xg[0, 0, 0, :, D:WIDE] = packed.astype(BF)
 
     pl.semaphore_wait(barrier, 10)
 
@@ -128,8 +113,29 @@
     def arrive(*key):
         copies[key].wait_recv()
 
+    def drain(*kinds):
+        for key in copies:
+            if key[0] in kinds:
+                copies[key].wait_send()
+
     near = (1, 3, 2)
     for part in range(3):
+        if part == 2:
+            lane = lax.broadcasted_iota(jnp.int32, (16, 128), 1)
+            ids = jnp.where(live, meta_a[...], -1.0)
+            gate = meta_b[...]
+            high = gate.astype(BF).astype(F32)
+            low = gate - high
+            packed = jnp.where(
+                lane < 8,
+                ids,
+                jnp.where(
+                    lane < 16,
+                    pltpu.roll(high, 8, 1),
+                    jnp.where(lane < 24, pltpu.roll(low, 16, 1), 0.0),
+                ),
+            )
+            xg[0, 0, 0, :, D:WIDE] = packed.astype(BF)
         for o in near:
             send(("a0", part, o), block(xg, part, 0, 0, 0), block(xg, part, 4 - o, 0, 0), part, o)
     for part in range(3):
@@ -252,6 +258,10 @@
         send(("r2l", 1, o), s1b.at[0, o], r2b.at[o - 1, 0], 2, o)
         send(("r2l", 0, o), s1a.at[0, o], r2a.at[o - 1, 0], 1, o)
 
+    drain("a0", "a1o", "a1", "a2l", "a2")
+    for n in range(3):
+        swap(n, mine).wait_send()
+
     for part in (2, 1, 0):
         for o in near:
             arrive("r1l", part, o)
@@ -273,6 +283,7 @@
         s2[part][1:4] = acc.astype(BF)
         for o in near:
             send(("r3", part, o), s2[part].at[o], r3[part].at[o - 1], part, o)
+    drain("r1", "r1l", "r2", "r2l")
     for part in (2, 1, 0):
         for o in near:
             arrive("r2l", part, o)
@@ -291,10 +302,7 @@
     mixed = mixed.astype(BF)
     for s in range(4):
         out_ref[s] = mixed[4 * s : 4 * s + 4, :]
-    for copy in copies.values():
-        copy.wait_send()
-    for n in range(3):
-        swap(n, mine).wait_send()
+    drain("r3")
 
 
 def per_device(

time: 45.8 us -> 45.6 us (level)
  no operation moved by 1% of the time
where the time goes in v5:
time: 45.6 us; the launch traced here: 45.5 us
  Pallas kernels  44.1 us (97%)
  local copies, waits for them, and re-layouts  1.39 us (3%)
    pallas_call x1, Pallas kernels, per_device(): pl.pallas_call(kernel, out_shape=jax.ShapeDtypeStruct(tokens.shape, BF),...  44.1 us
    unnamed x1, local copies, waits for them, and re-layouts  1.39 us

profile of v5, /device:TPU:0, one launch (start us, length us, event | category | flops | bytes accessed | tf_op | source)
XLA Modules:
  0.0 45.5 jit_solution(16520395993691203264)
XLA Ops:
  0.0 44.1 %shard_map.118 = bf16[4,4,1024]{2,1,0:T(4,128)(2,1)} custom-call(s32[4]{0:T(128)} %lengths_hbm.1, bf16[4,4,1024]{2,1,0:T(4,128)(2,1)} %tokens_hbm.1, s32[4,4,8]{2,1,0:T(4,128)} %routes_hbm.1, f32[4,4,8]{2,1,0:T(4,128)} %gates_hbm.1, f32[1,1024]{1,0:T(1,128)} %bitcast.2, f32[1,1024]{1,0:T(1,128)} %bitcast.3, bf16[2,1024,256]{2,1,0:T(8,128)(2,1)} %eg_ref.1, ...), custom_call_target="tpu_custom_call" | custom-call | tf_op jit(solution)/shard_map/pallas_call | solution.py:330
  44.1 1.4 %copy.14 = bf16[4,4,1024]{2,1,0:T(4,128)(2,1)} copy(bf16[4,4,1024]{2,1,0:T(4,128)(2,1)} %shard_map.118) | data formatting | bytes 65536

commit v6 on v5

--- a/solution.py
+++ b/solution.py
@@ -58,32 +58,24 @@
         copy.start()
         early.append(copy)
     mine = pl.ds(2 * core, 2)
-    local = []
-    for n, (src, dst) in enumerate(
-        (
-            (eg_ref, wg.at[mine]), (eu_ref, wu.at[mine]), (ed_ref, wd.at[mine]),
-            (sg_ref, sgv), (su_ref, suv), (sd_ref, sdv),
-        )
-    ):
-        copy = pltpu.make_async_copy(src, dst, w_local.at[n])
-        copy.start()
-        local.append(copy)
-
-    for copy in early:
-        copy.wait()
     row = lax.broadcasted_iota(jnp.int32, (16, 1), 0)
-    limit = jnp.zeros((16, 1), jnp.int32)
+    early[0].wait()
+    early[1].wait()
     for s in range(4):
-        limit = jnp.where(row // 4 == s, lengths_ref[s], limit)
         rows[4 * s : 4 * s + 4, :] = tokens_ref[s].astype(F32)
-        meta_a[4 * s : 4 * s + 4, 0:8] = routes_ref[s].astype(F32)
-        meta_b[4 * s : 4 * s + 4, 0:8] = gates_ref[s]
-    live = lax.rem(row, 4) < limit
     values = rows[...]
     mean = jnp.mean(values * values, axis=-1, keepdims=True)
     normed = (values * lax.rsqrt(mean + EPS) * ng_ref[...]).astype(BF)
     xg[0, 0, 0, :, 0:D] = normed
 
+    for copy in early[2:]:
+        copy.wait()
+    limit = jnp.zeros((16, 1), jnp.int32)
+    for s in range(4):
+        limit = jnp.where(row // 4 == s, lengths_ref[s], limit)
+        meta_a[4 * s : 4 * s + 4, 0:8] = routes_ref[s].astype(F32)
+        meta_b[4 * s : 4 * s + 4, 0:8] = gates_ref[s]
+    live = lax.rem(row, 4) < limit
     pl.semaphore_wait(barrier, 10)
 
     def swap(n, dst_slot):
@@ -143,6 +135,17 @@
             send(
                 ("a1o", part, o), block(xg, part, 0, 0, 0), block(xg, part, 0, 4 - o, 0), part + 1, o
             )
+    local = []
+    for n, (src, dst) in enumerate(
+        (
+            (eg_ref, wg.at[mine]), (eu_ref, wu.at[mine]), (ed_ref, wd.at[mine]),
+            (sg_ref, sgv), (su_ref, suv), (sd_ref, sdv),
+        )
+    ):
+        copy = pltpu.make_async_copy(src, dst, w_local.at[n])
+        copy.start()
+        local.append(copy)
+
     for n in range(3):
         swap(n, mine).start()
     for part in range(3):

time: 45.6 us -> 45.1 us (0.989)
  Pallas kernels: 44.1 us -> 43.5 us
    pallas_call x1, Pallas kernels: 44.1 us -> 43.5 us  [per_device(): pl.pallas_call(kernel, out_shape=jax.ShapeDtypeStruct(tokens.shape, BF),...]
where the time goes in v6:
time: 45.1 us; the launch traced here: 44.9 us
  Pallas kernels  43.5 us (96%)
  local copies, waits for them, and re-layouts  1.39 us (3%)
    pallas_call x1, Pallas kernels, per_device(): pl.pallas_call(kernel, out_shape=jax.ShapeDtypeStruct(tokens.shape, BF),...  43.5 us
    unnamed x1, local copies, waits for them, and re-layouts  1.39 us

profile of v6, /device:TPU:0, one launch (start us, length us, event | category | flops | bytes accessed | tf_op | source)
XLA Modules:
  0.0 44.9 jit_solution(8985330306744014929)
XLA Ops:
  0.0 43.5 %shard_map.118 = bf16[4,4,1024]{2,1,0:T(4,128)(2,1)} custom-call(s32[4]{0:T(128)} %lengths_hbm.1, bf16[4,4,1024]{2,1,0:T(4,128)(2,1)} %tokens_hbm.1, s32[4,4,8]{2,1,0:T(4,128)} %routes_hbm.1, f32[4,4,8]{2,1,0:T(4,128)} %gates_hbm.1, f32[1,1024]{1,0:T(1,128)} %bitcast.2, f32[1,1024]{1,0:T(1,128)} %bitcast.3, bf16[2,1024,256]{2,1,0:T(8,128)(2,1)} %eg_ref.1, ...), custom_call_target="tpu_custom_call" | custom-call | tf_op jit(solution)/shard_map/pallas_call | solution.py:333
  43.5 1.4 %copy.14 = bf16[4,4,1024]{2,1,0:T(4,128)(2,1)} copy(bf16[4,4,1024]{2,1,0:T(4,128)(2,1)} %shard_map.118) | data formatting | bytes 65536

commit v7 on v6

--- a/solution.py
+++ b/solution.py
@@ -40,12 +40,12 @@
     ]
 
     barrier = pltpu.get_barrier_semaphore()
-    pl.semaphore_signal(barrier, inc=1, device_id=(partner,), device_id_type=MESH)
-    for dim in range(3):
-        for o in (1, 2, 3):
+    for o in (2, 3, 1):
+        for dim in range(3):
             pl.semaphore_signal(
                 barrier, inc=1, device_id=(peers[dim][o],), device_id_type=MESH
             )
+    pl.semaphore_signal(barrier, inc=1, device_id=(partner,), device_id_type=MESH)
 
     early = []
     for n, (src, dst) in enumerate(
@@ -179,11 +179,6 @@
 
     for copy in local:
         copy.wait()
-    own = xg[0, 0, 0, :, 0:D]
-    part_g = jnp.dot(own, sgv[...], preferred_element_type=F32)
-    part_u = jnp.dot(own, suv[...], preferred_element_type=F32)
-    hidden = (part_g / (1.0 + jnp.exp(-part_g)) * part_u).astype(BF)
-    total[...] = jnp.dot(hidden, sdv[...], preferred_element_type=F32)
 
     for n in range(3):
         swap(n, theirs).wait_recv()
@@ -226,10 +221,12 @@
                 send(("r1", 2, k, o), out_block(2, ALL, k, o), r1c.at[o - 1, k], 1, o)
         if k != 0:
             send(("r1", 1, k), out_block(1, ALL, REST, k), r1b.at[k - 1, :, REST], 0, k)
+            send(("r1l", 1, k), out_block(1, ALL, 0, k), r1b.at[k - 1, :, 0], 0, k)
+        if k == 3:
+            for o in near:
+                send(("r1l", 2, o), out_block(2, ALL, 0, o), r1c.at[o - 1, 0], 1, o)
     for o in near:
         send(("r1l", 0, o), out_block(0, ALL, 0, o), r1a.at[o - 1, :, 0], 2, o)
-        send(("r1l", 1, o), out_block(1, ALL, 0, o), r1b.at[o - 1, :, 0], 0, o)
-        send(("r1l", 2, o), out_block(2, ALL, 0, o), r1c.at[o - 1, 0], 1, o)
 
     for k in (1, 3, 2):
         for o in near:
@@ -261,6 +258,11 @@
         send(("r2l", 1, o), s1b.at[0, o], r2b.at[o - 1, 0], 2, o)
         send(("r2l", 0, o), s1a.at[0, o], r2a.at[o - 1, 0], 1, o)
 
+    own = xg[0, 0, 0, :, 0:D]
+    part_g = jnp.dot(own, sgv[...], preferred_element_type=F32)
+    part_u = jnp.dot(own, suv[...], preferred_element_type=F32)
+    hidden = (part_g / (1.0 + jnp.exp(-part_g)) * part_u).astype(BF)
+    total[...] = jnp.dot(hidden, sdv[...], preferred_element_type=F32)
     drain("a0", "a1o", "a1", "a2l", "a2")
     for n in range(3):
         swap(n, mine).wait_send()

time: 45.1 us -> 45 us (level)
  no operation moved by 1% of the time
where the time goes in v7:
time: 45 us; the launch traced here: 44.8 us
  Pallas kernels  43.4 us (96%)
  local copies, waits for them, and re-layouts  1.39 us (3%)
    pallas_call x1, Pallas kernels, per_device(): pl.pallas_call(kernel, out_shape=jax.ShapeDtypeStruct(tokens.shape, BF),...  43.4 us
    unnamed x1, local copies, waits for them, and re-layouts  1.39 us

profile of v7, /device:TPU:0, one launch (start us, length us, event | category | flops | bytes accessed | tf_op | source)
XLA Modules:
  0.0 44.8 jit_solution(11758525488573645490)
XLA Ops:
  0.0 43.4 %shard_map.118 = bf16[4,4,1024]{2,1,0:T(4,128)(2,1)} custom-call(s32[4]{0:T(128)} %lengths_hbm.1, bf16[4,4,1024]{2,1,0:T(4,128)(2,1)} %tokens_hbm.1, s32[4,4,8]{2,1,0:T(4,128)} %routes_hbm.1, f32[4,4,8]{2,1,0:T(4,128)} %gates_hbm.1, f32[1,1024]{1,0:T(1,128)} %bitcast.2, f32[1,1024]{1,0:T(1,128)} %bitcast.3, bf16[2,1024,256]{2,1,0:T(8,128)(2,1)} %eg_ref.1, ...), custom_call_target="tpu_custom_call" | custom-call | tf_op jit(solution)/shard_map/pallas_call | solution.py:335
  43.4 1.4 %copy.14 = bf16[4,4,1024]{2,1,0:T(4,128)(2,1)} copy(bf16[4,4,1024]{2,1,0:T(4,128)(2,1)} %shard_map.118) | data formatting | bytes 65536

commit v8 on v7

--- a/solution.py
+++ b/solution.py
@@ -39,14 +39,6 @@
         for dim in range(3)
     ]
 
-    barrier = pltpu.get_barrier_semaphore()
-    for o in (2, 3, 1):
-        for dim in range(3):
-            pl.semaphore_signal(
-                barrier, inc=1, device_id=(peers[dim][o],), device_id_type=MESH
-            )
-    pl.semaphore_signal(barrier, inc=1, device_id=(partner,), device_id_type=MESH)
-
     early = []
     for n, (src, dst) in enumerate(
         (
@@ -57,6 +49,14 @@
         copy = pltpu.make_async_copy(src, dst, small.at[n])
         copy.start()
         early.append(copy)
+
+    barrier = pltpu.get_barrier_semaphore()
+    for o in (2, 3, 1):
+        for dim in range(3):
+            pl.semaphore_signal(
+                barrier, inc=1, device_id=(peers[dim][o],), device_id_type=MESH
+            )
+    pl.semaphore_signal(barrier, inc=1, device_id=(partner,), device_id_type=MESH)
     mine = pl.ds(2 * core, 2)
     row = lax.broadcasted_iota(jnp.int32, (16, 1), 0)
     early[0].wait()

time: 45 us -> 45 us (level)
  no operation moved by 1% of the time
where the time goes in v8:
time: 45 us; the launch traced here: 44.8 us
  Pallas kernels  43.4 us (96%)
  local copies, waits for them, and re-layouts  1.39 us (3%)
    pallas_call x1, Pallas kernels, per_device(): pl.pallas_call(kernel, out_shape=jax.ShapeDtypeStruct(tokens.shape, BF),...  43.4 us
    unnamed x1, local copies, waits for them, and re-layouts  1.39 us

profile of v8, /device:TPU:0, one launch (start us, length us, event | category | flops | bytes accessed | tf_op | source)
XLA Modules:
  0.0 44.8 jit_solution(5118943814369460869)
XLA Ops:
  0.0 43.4 %shard_map.118 = bf16[4,4,1024]{2,1,0:T(4,128)(2,1)} custom-call(s32[4]{0:T(128)} %lengths_hbm.1, bf16[4,4,1024]{2,1,0:T(4,128)(2,1)} %tokens_hbm.1, s32[4,4,8]{2,1,0:T(4,128)} %routes_hbm.1, f32[4,4,8]{2,1,0:T(4,128)} %gates_hbm.1, f32[1,1024]{1,0:T(1,128)} %bitcast.2, f32[1,1024]{1,0:T(1,128)} %bitcast.3, bf16[2,1024,256]{2,1,0:T(8,128)(2,1)} %eg_ref.1, ...), custom_call_target="tpu_custom_call" | custom-call | tf_op jit(solution)/shard_map/pallas_call | solution.py:335
  43.4 1.4 %copy.14 = bf16[4,4,1024]{2,1,0:T(4,128)(2,1)} copy(bf16[4,4,1024]{2,1,0:T(4,128)(2,1)} %shard_map.118) | data formatting | bytes 65536
